TPU v7x, 32 devices: a whole 2x2x4 slice. The times are simulated.
32 devices in a mesh: ep: 8 (over z, core), tp: 4 (over y, x).
Axes of the slice: x: 2, y: 2, z: 4, core: 2. Of those that a mesh axis runs over, the one named last changes fastest.
Arguments:
- tokens: bfloat16 [1024, 2048], P('ep'), may hold values from -6 to 6
- selected: int32 [8, 256], P(None, 'ep'), may hold values from -1 to 127, as said below
- affinity: float32 [8, 256], P(None, 'ep'), may hold values from 0.05 to 1
- w_gate: bfloat16 [8, 2048, 2048], P('ep', None, 'tp'), may hold values from -0.125 to 0.125
- w_up: bfloat16 [8, 2048, 2048], P('ep', None, 'tp'), may hold values from -0.125 to 0.125
- w_down: bfloat16 [8, 2048, 2048], P('ep', 'tp'), may hold values from -0.125 to 0.125
Outputs:
- combined: bfloat16 [1024, 2048], P('ep', 'tp')
Inputs may be any that keep to these rules, and one draw needn't show every extreme that they name: `selected`: row e holds 8 aligned groups of 32 entries; the live entries of group j are distinct positions within the j-th block of 128 tokens, stand at the front of the group and are followed by -1; each row has 128 live entries in all, the number in a group varies, and some group of every row is full.
All inputs are finite; a program needn't handle non-finite values.
Results may differ from a plain program's by a relative error of at most 0.015.
Values may be sent and summed in bfloat16 or wider, within the bound.
A program may use at most 64 MiB of HBM per device.

v0:
```python
import jax
import jax.numpy as jnp
from jax import lax
from jax.sharding import PartitionSpec as P


def per_device(tokens, selected, affinity, w_gate, w_up, w_down):
    ep_count = lax.axis_size("ep")
    local_tokens = tokens.shape[0]
    experts_here = w_gate.shape[0]
    slot_count = selected.shape[1]
    clamped = jnp.maximum(selected, 0)
    gathered = jnp.take(tokens, clamped, axis=0)
    arrived = lax.all_to_all(gathered, "ep", split_axis=0, concat_axis=1, tiled=True)
    gate_act = jnp.einsum("ecd,edf->ecf", arrived, w_gate, preferred_element_type=jnp.float32)
    up_act = jnp.einsum("ecd,edf->ecf", arrived, w_up, preferred_element_type=jnp.float32)
    hidden = (jax.nn.silu(gate_act) * up_act).astype(jnp.bfloat16)
    summed = lax.psum_scatter(
        jnp.einsum("efd,ecf->dec", w_down, hidden, preferred_element_type=jnp.float32).astype(
            jnp.bfloat16
        ),
        "tp",
        scatter_dimension=0,
        tiled=True,
    )
    summed = summed.reshape(summed.shape[0], experts_here, ep_count, slot_count)
    returned = lax.all_to_all(summed, "ep", split_axis=2, concat_axis=1, tiled=True)
    feature_cols = returned.shape[0]
    returned = returned.reshape(feature_cols, experts_here * ep_count * slot_count)
    weights = jnp.where(selected >= 0, affinity, jnp.zeros_like(affinity)).reshape(-1)
    scaled_rows = returned.astype(jnp.float32).T * weights[:, None]
    combined = (
        jnp.zeros((local_tokens, feature_cols), jnp.float32)
        .at[clamped.reshape(-1)]
        .add(scaled_rows)
    )
    return combined.astype(jnp.bfloat16)


def solution(mesh):
    placed = (
        P("ep", None),
        P(None, "ep"),
        P(None, "ep"),
        P("ep", None, "tp"),
        P("ep", None, "tp"),
        P("ep", "tp", None),
    )
    return jax.shard_map(
        per_device, mesh=mesh, in_specs=placed, out_specs=P("ep", "tp"), check_vma=False
    )
```

profile of v0, /device:TPU:0, one launch (start us, length us, event | category | flops | bytes accessed | tf_op | source)
XLA Modules:
  0.0 101.5 jit_solution(7033173364249277879)
XLA Ops:
  6.5 0.0 copy-start
  6.5 0.0 reduce-scatter.2.cloned.1.call-start
  6.5 0.8 broadcast_maximum_fusion
  7.4 0.7 broadcast_compare_fusion
  8.1 0.1 reshape.87
  8.2 3.5 %gather_fusion = bf16[256,2048]{1,0:T(8,128)(2,1)S(1)} fusion(bf16[128,2048]{1,0:T(8,128)(2,1)} %param.6, s32[1024]{0:T(1024)S(1)} %pad_clamp_fusion), kind=kCustom, calls=%fused_computation | custom fusion | bytes 2098176 | tf_op jit(solution)/shard_map/jit(_take)/gather | solution.py:13
  11.6 0.0 copy-start.3
  11.6 0.2 broadcast_select_fusion
  11.8 32.8 %all_to_all.8 = bf16[8,32,2048]{2,1,0:T(8,128)(2,1)S(1)} all-to-all(bf16[8,32,2048]{2,1,0:T(8,128)(2,1)S(1)} %broadcast_select_fusion), channel_id=1, replica_groups=mesh['ep'=8,'tp'=4] {'ep'}, dimensions={0} | all-to-all | bytes 2097152 | tf_op jit(solution)/shard_map/all_to_all | solution.py:14
  44.7 0.0 copy-done.3
  44.7 1.6 %fusion.4 = f32[256,512]{1,0:T(8,128)} fusion(bf16[256,2048]{1,0:T(8,128)(2,1)S(1)} %bitcast.34, bf16[1,2048,512]{2,1,0:T(8,128)(2,1)S(1)} %copy-done.3), kind=kOutput, calls=%fused_computation.7 | convolution fusion | flops 536870912 | bytes 3670016 | tf_op jit(solution)/shard_map/ecd,edf->ecf/dot_general | solution.py:15
  46.2 0.0 copy-done
  46.2 0.0 copy-start.1
  46.2 0.0 copy-start.2
  46.2 4.0 %fusion = bf16[2048,1,256]{0,2,1:T(8,128)(2,1)} fusion(bf16[1,512,2048]{2,1,0:T(8,128)(2,1)S(1)} %copy-done, bf16[256,2048]{1,0:T(8,128)(2,1)S(1)} %bitcast.35, bf16[1,2048,512]{2,1,0:T(8,128)(2,1)} %param.10, f32[256,512]{1,0:T(8,128)} %fusion.4), kind=kOutput, calls=%fused_computation.3 | convolution fusion | flops 1075052544 | bytes 6815744 | tf_op jit(solution)/shard_map/efd,ecf->dec/dot_general | solution.py:19
  50.3 0.0 reduce-scatter.2.cloned.1.call-update
  50.3 27.0 %reduce-scatter.2.cloned.1.call-done = bf16[512,1,256]{0,2,1:T(8,128)(2,1)} async-done(((bf16[2048,1,256]{0,2,1:T(8,128)(2,1)}), bf16[512,1,256]{0,2,1:T(8,128)(2,1)}) %reduce-scatter.2.cloned.1.call-update) | async-done | bytes 262160 | tf_op jit(solution)/shard_map/reduce_scatter | solution.py:18
  77.3 4.6 %all-to-all-start.1 = ((bf16[512,1,8,32]{0,3,1,2:T(8,128)(2,1)}), bf16[512,1,8,32]{0,3,1,2:T(8,128)(2,1)S(1)}, u32[]{:S(2)}, u32[]{:S(2)}) async-start(bf16[512,1,8,32]{0,3,1,2:T(8,128)(2,1)} %bitcast.36), calls=%async_computation.2 | async-start | bytes 524288 | tf_op jit(solution)/shard_map/all_to_all | solution.py:27
  81.9 0.1 reshape.78
  82.0 0.0 copy-done.1
  82.0 0.0 copy-done.2
  82.0 0.1 mul.24
  82.1 9.5 %all-to-all-done.1 = bf16[512,1,8,32]{0,3,1,2:T(8,128)(2,1)S(1)} async-done(((bf16[512,1,8,32]{0,3,1,2:T(8,128)(2,1)}), bf16[512,1,8,32]{0,3,1,2:T(8,128)(2,1)S(1)}, u32[]{:S(2)}, u32[]{:S(2)}) %all-to-all-start.1) | async-done | bytes 262176 | tf_op jit(solution)/shard_map/all_to_all | solution.py:27
  91.6 2.3 %scatter_custom_fusion = f32[128,512]{1,0:T(8,128)S(1)} fusion(s32[256]{0:T(256)S(1)} %bitcast.37, bf16[512,256]{0,1:T(8,128)(2,1)S(1)} %bitcast.33, f32[256]{0:T(256)S(1)} %mul.24, f32[]{:T(128)} %constant.9.clone.1), kind=kCustom, calls=%fused_computation.14 | custom fusion | flops 393216 | bytes 525316 | tf_op jit(solution)/shard_map/scatter-add | solution.py:35
  94.0 0.7 convert_element_type.28
  (3 shorter events, 0.0 us)
Async XLA Ops:
  6.5 39.7 %copy-start = (bf16[1,512,2048]{2,1,0:T(8,128)(2,1)S(1)}, bf16[1,512,2048]{2,1,0:T(8,128)(2,1)}, u32[]{:S(2)}) copy-start(bf16[1,512,2048]{2,1,0:T(8,128)(2,1)} %param.11) | copy-start | bytes 6291460
  6.5 70.8 %reduce-scatter.2.cloned.1.call-start = ((), (), s32[]{:S(2)}) async-start(), calls=%async_computation.3 | async-start | bytes 1310720 | tf_op jit(solution)/shard_map/reduce_scatter | solution.py:18
  11.6 33.0 %copy-start.3 = (bf16[1,2048,512]{2,1,0:T(8,128)(2,1)S(1)}, bf16[1,2048,512]{2,1,0:T(8,128)(2,1)}, u32[]{:S(2)}) copy-start(bf16[1,2048,512]{2,1,0:T(8,128)(2,1)} %param.9) | copy-start | bytes 6291460
  46.2 35.8 %copy-start.1 = (s32[8,32]{1,0:T(8,128)S(1)}, s32[8,32]{1,0:T(8,128)}, u32[]{:S(2)}) copy-start(s32[8,32]{1,0:T(8,128)} %param.7) | copy-start | bytes 3076
  46.2 35.8 %copy-start.2 = (f32[8,32]{1,0:T(8,128)S(1)}, f32[8,32]{1,0:T(8,128)}, u32[]{:S(2)}) copy-start(f32[8,32]{1,0:T(8,128)} %param.8) | copy-start | bytes 3076
  77.3 14.3 %all-to-all-start.1 = ((bf16[512,1,8,32]{0,3,1,2:T(8,128)(2,1)}), bf16[512,1,8,32]{0,3,1,2:T(8,128)(2,1)S(1)}, u32[]{:S(2)}, u32[]{:S(2)}) async-start(bf16[512,1,8,32]{0,3,1,2:T(8,128)(2,1)} %bitcast.36), calls=%async_computation.2 | async-start | bytes 524288 | tf_op jit(solution)/shard_map/all_to_all | solution.py:27
Sparse Core Ops, SparseCore 0:
  50.4 26.8 reduce-scatter.1
where the time goes:
time: 102 us; the launch traced here: 101 us
  waiting for transfers between devices  36.6 us (36%)
  blocking collectives  32.8 us (32%)
  between operations  13.4 us (13%)
  matrix products  5.59 us (5%)
  other arithmetic  4.72 us (5%)
  starting transfers between devices  4.62 us (5%)
  local copies, waits for them, and re-layouts  3.73 us (4%)
    all_to_all x1, blocking collectives, per_device(): lax.all_to_all(gathered, 'ep', split_axis=0, concat_axis=1, tiled=True)  32.8 us
    reduce_scatter x1, waiting for transfers between devices, per_device(): lax.psum_scatter(jnp.einsum('efd,ecf->dec', w_down, hidden, preferred_ele...  27 us
    all_to_all x1, waiting for transfers between devices, per_device(): lax.all_to_all(summed, 'ep', split_axis=2, concat_axis=1, tiled=True)  9.54 us
    all_to_all x1, starting transfers between devices, per_device(): lax.all_to_all(summed, 'ep', split_axis=2, concat_axis=1, tiled=True)  4.61 us
    dot_general x1, matrix products, per_device(): jnp.einsum('efd,ecf->dec', w_down, hidden, preferred_element_type=jnp.flo...  4.04 us
    gather x1, local copies, waits for them, and re-layouts, per_device(): gathered = jnp.take(tokens, clamped, axis=0)  3.48 us
    scatter-add x1, other arithmetic, per_device(): combined = jnp.zeros((local_tokens, feature_cols), jnp.float32).at[clampe...  2.34 us
  transfers between devices with their start and end apart: 2, of which 2 were waited for; matrix products, arithmetic and copies ran while one was open for 0% of the time, Pallas kernels for 0%

commit v1 on v0

v1 whole, which is shorter than its diff:
```python
import functools
import math

import jax
import jax.numpy as jnp
from jax import lax
from jax.experimental import pallas as pl
from jax.experimental.pallas import tpu as pltpu
from jax.sharding import PartitionSpec as P

MESH = pl.DeviceIdType.MESH
F32 = jnp.float32
BF16 = jnp.bfloat16
CHUNK = 256


def side_of(n):
    s = math.isqrt(n)
    while n % s:
        s -= 1
    return s


def kernel(
    n_ep, n_tp, chunks,
    tok_hbm, sel_hbm, aff_hbm, wg_hbm, wu_hbm, wd_hbm, out_ref,
    tok, sel, aff, wgu, wd, onehot, weight_hi, weight_lo, expand, compact,
    cnt_out, cnt_in, z_out, z_in, rows, acc, hid, part_out, part_in, ret_out, ret_in,
    s_in, s_wg, s_wu, s_wd, s_cnt_s, s_cnt_r, s_z_s, s_z_r, s_x_s, s_x_r,
    s_p_s, s_p_r, s_r_s, s_r_r,
):
    ep = lax.axis_index("ep")
    tp = lax.axis_index("tp")
    n_tok, feats = tok.shape
    n_exp, group = sel.shape
    fc = feats // chunks
    live = rows.shape[2]
    hidden = hid.shape[1]

    width = side_of(n_tp)
    height = n_tp // width
    y, x = tp // width, lax.rem(tp, width)
    offsets = [(dy, dx) for dy in range(height) for dx in range(width)][1:]
    near = sorted(offsets, key=lambda o: (o[0] > 0) + (o[1] > 0))
    far = near[::-1]

    def tp_to(o):
        return lax.rem(y + o[0], height) * width + lax.rem(x + o[1], width)

    def tp_from(o):
        return lax.rem(y + height - o[0], height) * width + lax.rem(x + width - o[1], width)

    def tp_sem(o):
        return o[0] * width + o[1]

    ep_order = sorted(range(1, n_ep), key=lambda d: (abs(d - n_ep / 2), d))

    def ep_to(d):
        return lax.rem(ep + d, n_ep)

    def rows_of(i):
        return pl.ds(pl.multiple_of(i * group, group), group)

    load_sel = pltpu.make_async_copy(sel_hbm, sel, s_in.at[0])
    load_tok = pltpu.make_async_copy(
        tok_hbm.at[:, pl.ds(pl.multiple_of(tp * feats, 128), feats)], tok, s_in.at[1]
    )
    load_aff = pltpu.make_async_copy(aff_hbm, aff, s_in.at[2])
    load_sel.start()
    load_tok.start()

    barrier = pltpu.get_barrier_semaphore()
    for d in ep_order:
        pl.semaphore_signal(barrier, inc=1, device_id={"ep": ep_to(d)}, device_id_type=MESH)
    for o in far:
        pl.semaphore_signal(barrier, inc=1, device_id={"tp": tp_to(o)}, device_id_type=MESH)

    load_aff.start()
    load_w = []
    for k in range(n_tp):
        for c in range(chunks):
            at = pl.ds(k * feats + c * fc, fc)
            load_w.append(pltpu.make_async_copy(
                wg_hbm.at[0, at, :], wgu.at[k, c, :, pl.ds(0, hidden)], s_wg.at[k, c]))
            load_w.append(pltpu.make_async_copy(
                wu_hbm.at[0, at, :], wgu.at[k, c, :, pl.ds(hidden, hidden)], s_wu.at[k, c]))
    load_d = [
        pltpu.make_async_copy(
            wd_hbm.at[0, :, pl.ds(k * feats, feats)], wd.at[k], s_wd.at[k])
        for k in range(n_tp)
    ]
    for copy in load_w + load_d:
        copy.start()

    load_sel.wait()
    picked = sel[...].astype(F32)
    count = jnp.sum(jnp.where(picked >= 0, 1.0, 0.0), axis=1, keepdims=True)
    for e in range(n_exp):
        cnt_out[e] = jnp.broadcast_to(count[e:e + 1, :], (8, 128))
    picked_t = jnp.transpose(picked)
    token_lane = lax.broadcasted_iota(jnp.int32, (group, n_tok), 1).astype(F32)
    for e in range(n_exp):
        onehot[pl.ds(e * group, group), :] = jnp.where(
            picked_t[:, e:e + 1] == token_lane, 1.0, 0.0)
    load_tok.wait()
    pick = onehot[...].astype(BF16)
    for c in range(chunks):
        z_out[c] = jnp.dot(
            pick, tok[:, c * fc:(c + 1) * fc], preferred_element_type=F32).astype(BF16)
        z_in[c, rows_of(ep), :] = z_out[c, rows_of(ep), :]
    cnt_in[ep] = cnt_out[ep]

    pl.semaphore_wait(barrier, len(ep_order) + len(far))

    sent = []
    cnt_copy = {}
    z_copy = {}

    def send(src, dst, ss, rs, to):
        copy = pltpu.make_async_remote_copy(
            src_ref=src, dst_ref=dst, send_sem=ss, recv_sem=rs,
            device_id=to, device_id_type=MESH)
        copy.start()
        sent.append(copy)
        return copy

    for c in range(chunks):
        for d in ep_order:
            z_copy[c, d] = send(
                z_out.at[c, rows_of(ep_to(d)), :], z_in.at[c, rows_of(ep), :],
                s_z_s.at[c, d], s_z_r.at[c, d], {"ep": ep_to(d)})
            if c == 0:
                cnt_copy[d] = send(
                    cnt_out.at[ep_to(d)], cnt_in.at[ep],
                    s_cnt_s.at[d], s_cnt_r.at[d], {"ep": ep_to(d)})

    load_aff.wait()
    aff_t = jnp.transpose(aff[...])
    for e in range(n_exp):
        at = pl.ds(e * group, group)
        onehot[at, :] = onehot[at, :] * aff_t[:, e:e + 1]
    weight = jnp.transpose(onehot[...])
    high = weight.astype(BF16)
    weight_hi[...] = high
    weight_lo[...] = (weight - high.astype(F32)).astype(BF16)

    for copy in load_w:
        copy.wait()

    for d in ep_order:
        cnt_copy[d].wait_recv()
    lane = lax.broadcasted_iota(jnp.int32, (group, live), 1).astype(F32)
    row = lax.broadcasted_iota(jnp.int32, (group, live), 0).astype(F32)
    start = jnp.zeros((group, live), F32)
    pieces = []
    for j in range(n_ep):
        n = jnp.broadcast_to(cnt_in[j, 0:1, 0:1], (group, live))
        pieces.append(jnp.where((lane - row == start) & (row < n), 1.0, 0.0))
        start = start + n
    spread = jnp.concatenate(pieces, axis=0)
    expand[...] = spread.astype(BF16)
    compact[...] = jnp.transpose(spread).astype(BF16)

    acc[...] = jnp.zeros_like(acc)
    x_copy = {}

    def take(c, k):
        acc[...] += jnp.dot(rows[c, k], wgu[k, c], preferred_element_type=F32)

    def arrivals(c):
        for o in near:
            x_copy[c, o].wait_recv()
            take(c, tp_from(o))

    for c in range(chunks):
        for d in ep_order:
            z_copy[c, d].wait_recv()
        rows[c, tp] = jnp.dot(
            compact[...], z_in[c], preferred_element_type=F32).astype(BF16)
        for o in far:
            x_copy[c, o] = send(
                rows.at[c, tp], rows.at[c, tp],
                s_x_s.at[c, tp_sem(o)], s_x_r.at[c, tp_sem(o)], {"tp": tp_to(o)})
        take(c, tp)
        if c > 0:
            arrivals(c - 1)
    arrivals(chunks - 1)

    gate = acc[:, :hidden]
    up = acc[:, hidden:]
    hid[...] = (gate / (1.0 + jnp.exp(-gate)) * up).astype(BF16)

    for copy in load_d:
        copy.wait()

    p_copy = {}
    for c in range(chunks):
        for o in far + [(0, 0)]:
            k = tp_to(o)
            part_out[c, k] = jnp.dot(
                hid[...], wd[k, :, c * fc:(c + 1) * fc], preferred_element_type=F32
            ).astype(BF16)
            if o != (0, 0):
                p_copy[c, o] = send(
                    part_out.at[c, k], part_in.at[c, tp],
                    s_p_s.at[c, tp_sem(o)], s_p_r.at[c, tp_sem(o)], {"tp": k})

    r_copy = {}
    for c in range(chunks):
        total = part_out[c, tp].astype(F32)
        for o in near:
            p_copy[c, o].wait_recv()
            total = total + part_in[c, tp_from(o)].astype(F32)
        ret_out[c] = jnp.dot(
            expand[...], total.astype(BF16), preferred_element_type=F32).astype(BF16)
        for d in ep_order:
            r_copy[c, d] = send(
                ret_out.at[c, rows_of(ep_to(d)), :], ret_in.at[c, rows_of(ep), :],
                s_r_s.at[c, d], s_r_r.at[c, d], {"ep": ep_to(d)})
        ret_in[c, rows_of(ep), :] = ret_out[c, rows_of(ep), :]

    for c in range(chunks):
        for d in ep_order:
            r_copy[c, d].wait_recv()
        back = ret_in[c]
        out_ref[:, c * fc:(c + 1) * fc] = (
            jnp.dot(weight_hi[...], back, preferred_element_type=F32)
            + jnp.dot(weight_lo[...], back, preferred_element_type=F32)
        ).astype(BF16)

    for copy in sent:
        copy.wait_send()


def per_device(tokens, selected, affinity, w_gate, w_up, w_down):
    n_ep = lax.axis_size("ep")
    n_tp = lax.axis_size("tp")
    n_tok, width = tokens.shape
    n_exp, group = selected.shape
    hidden = w_gate.shape[2]
    assert w_gate.shape[0] == 1 and n_exp == n_ep
    feats = width // n_tp
    chunks = max(1, feats // CHUNK)
    fc = feats // chunks
    slots = n_ep * group
    live = slots // 2
    dma = pltpu.SemaphoreType.DMA
    any_spec = pl.BlockSpec(memory_space=pl.ANY)
    return pl.pallas_call(
        functools.partial(kernel, n_ep, n_tp, chunks),
        out_shape=jax.ShapeDtypeStruct((n_tok, feats), BF16),
        in_specs=[any_spec] * 6,
        out_specs=pl.BlockSpec(memory_space=pltpu.VMEM),
        scratch_shapes=[
            pltpu.VMEM((n_tok, feats), BF16),
            pltpu.VMEM((n_exp, group), jnp.int32),
            pltpu.VMEM((n_exp, group), F32),
            pltpu.VMEM((n_tp, chunks, fc, 2 * hidden), BF16),
            pltpu.VMEM((n_tp, hidden, feats), BF16),
            pltpu.VMEM((slots, n_tok), F32),
            pltpu.VMEM((n_tok, slots), BF16),
            pltpu.VMEM((n_tok, slots), BF16),
            pltpu.VMEM((slots, live), BF16),
            pltpu.VMEM((live, slots), BF16),
            pltpu.VMEM((n_exp, 8, 128), F32),
            pltpu.VMEM((n_ep, 8, 128), F32),
            pltpu.VMEM((chunks, slots, fc), BF16),
            pltpu.VMEM((chunks, slots, fc), BF16),
            pltpu.VMEM((chunks, n_tp, live, fc), BF16),
            pltpu.VMEM((live, 2 * hidden), F32),
            pltpu.VMEM((live, hidden), BF16),
            pltpu.VMEM((chunks, n_tp, live, fc), BF16),
            pltpu.VMEM((chunks, n_tp, live, fc), BF16),
            pltpu.VMEM((chunks, slots, fc), BF16),
            pltpu.VMEM((chunks, slots, fc), BF16),
            dma((3,)),
            dma((n_tp, chunks)),
            dma((n_tp, chunks)),
            dma((n_tp,)),
            dma((n_ep,)),
            dma((n_ep,)),
            dma((chunks, n_ep)),
            dma((chunks, n_ep)),
            dma((chunks, n_tp)),
            dma((chunks, n_tp)),
            dma((chunks, n_tp)),
            dma((chunks, n_tp)),
            dma((chunks, n_ep)),
            dma((chunks, n_ep)),
        ],
        compiler_params=pltpu.CompilerParams(collective_id=0, has_side_effects=True),
    )(tokens, selected, affinity, w_gate, w_up, w_down)


def solution(mesh):
    placed = (
        P("ep", None),
        P(None, "ep"),
        P(None, "ep"),
        P("ep", None, "tp"),
        P("ep", None, "tp"),
        P("ep", "tp", None),
    )
    return jax.shard_map(
        per_device, mesh=mesh, in_specs=placed, out_specs=P("ep", "tp"), check_vma=False
    )
```

time: 102 us -> 37.2 us (0.36)
  waiting for transfers between devices: 36.6 us -> 0 us
  Pallas kernels: 0 us -> 35.4 us
  blocking collectives: 32.8 us -> 0 us
  between operations: 13.4 us -> 0.01 us
  matrix products: 5.59 us -> 0 us
  other arithmetic: 4.72 us -> 0 us
  starting transfers between devices: 4.62 us -> 0 us
  local copies, waits for them, and re-layouts: 3.73 us -> 1.57 us
    pallas_call x0 -> x1, Pallas kernels: none -> 35.4 us  [per_device(): pl.pallas_call(functools.partial(kernel, n_ep, n_tp, chunks), out_shape=j...]
    all_to_all x1 -> x0, blocking collectives: 32.8 us -> none  [per_device(): lax.all_to_all(gathered, 'ep', split_axis=0, concat_axis=1, tiled=True)]
    reduce_scatter x1 -> x0, waiting for transfers between devices: 27 us -> none  [per_device(): lax.psum_scatter(jnp.einsum('efd,ecf->dec', w_down, hidden, preferred_ele...]
    all_to_all x1 -> x0, waiting for transfers between devices: 9.54 us -> none  [per_device(): lax.all_to_all(summed, 'ep', split_axis=2, concat_axis=1, tiled=True)]
    dot_general x2 -> x0, matrix products: 5.59 us -> none  [the longest x1 4.04 us: per_device(): jnp.einsum('efd,ecf->dec', w_down, hidden, preferred_element_type=jnp.flo...]
    all_to_all x1 -> x0, starting transfers between devices: 4.61 us -> none  [per_device(): lax.all_to_all(summed, 'ep', split_axis=2, concat_axis=1, tiled=True)]
    gather x1 -> x0, local copies, waits for them, and re-layouts: 3.48 us -> none  [per_device(): gathered = jnp.take(tokens, clamped, axis=0)]
    scatter-add x1 -> x0, other arithmetic: 2.34 us -> none  [per_device(): combined = jnp.zeros((local_tokens, feature_cols), jnp.float32).at[clampe...]
  transfers between devices with their start and end apart: 2 -> 0, of which waited for: 2 -> 0; matrix products, arithmetic and copies ran while one was open for 0% -> 0% of each run, Pallas kernels for 0% -> 0%
where the time goes in v1:
time: 37.2 us; the launch traced here: 37 us
  Pallas kernels  35.4 us (95%)
  local copies, waits for them, and re-layouts  1.57 us (4%)
    pallas_call x1, Pallas kernels, per_device(): pl.pallas_call(functools.partial(kernel, n_ep, n_tp, chunks), out_shape=j...  35.4 us
    unnamed x1, local copies, waits for them, and re-layouts  1.57 us

profile of v1, /device:TPU:0, one launch (start us, length us, event | category | flops | bytes accessed | tf_op | source)
XLA Modules:
  0.0 37.0 jit_solution(15173019861656123475)
XLA Ops:
  0.0 35.4 %shard_map.64 = bf16[128,512]{1,0:T(8,128)(2,1)} custom-call(bf16[128,2048]{1,0:T(8,128)(2,1)} %tok_hbm.1, s32[8,32]{1,0:T(8,128)} %sel_hbm.1, f32[8,32]{1,0:T(8,128)} %aff_hbm.1, bf16[1,2048,512]{2,1,0:T(8,128)(2,1)} %wg_hbm.1, bf16[1,2048,512]{2,1,0:T(8,128)(2,1)} %wu_hbm.1, bf16[1,512,2048]{2,1,0:T(8,128)(2,1)} %wd_hbm.1), custom_call_target="tpu_custom_call" | custom-call | tf_op jit(solution)/shard_map/pallas_call | solution.py:249
  35.4 1.6 %copy.8 = bf16[128,512]{1,0:T(8,128)(2,1)} copy(bf16[128,512]{1,0:T(8,128)(2,1)} %shard_map.64) | data formatting | bytes 262144

commit v2 on v1

--- a/solution.py
+++ b/solution.py
@@ -11,7 +11,8 @@
 MESH = pl.DeviceIdType.MESH
 F32 = jnp.float32
 BF16 = jnp.bfloat16
-CHUNK = 256
+CHUNK = 128
+LAG = 2
 
 
 def side_of(n):
@@ -53,10 +54,17 @@
     def tp_sem(o):
         return o[0] * width + o[1]
 
-    ep_order = sorted(range(1, n_ep), key=lambda d: (abs(d - n_ep / 2), d))
-
-    def ep_to(d):
-        return lax.rem(ep + d, n_ep)
+    ep_order = list(range(n_ep - 1))
+    high_half = ep // (n_ep // 2)
+
+    def ep_to(i):
+        down = n_ep - 1 - i
+        down = down - jnp.where(down <= ep, 1, 0)
+        up = i + jnp.where(i >= ep, 1, 0)
+        return jnp.where(high_half > 0, up, down)
+
+    def ep_from(i):
+        return lax.rem(ep + 1 + i, n_ep)
 
     def rows_of(i):
         return pl.ds(pl.multiple_of(i * group, group), group)
@@ -113,8 +121,6 @@
     pl.semaphore_wait(barrier, len(ep_order) + len(far))
 
     sent = []
-    cnt_copy = {}
-    z_copy = {}
 
     def send(src, dst, ss, rs, to):
         copy = pltpu.make_async_remote_copy(
@@ -124,15 +130,20 @@
         sent.append(copy)
         return copy
 
+    def arrived(dst, rs):
+        pltpu.make_async_remote_copy(
+            src_ref=dst, dst_ref=dst, send_sem=s_in.at[0], recv_sem=rs,
+            device_id={"ep": ep_from(0)}, device_id_type=MESH).wait_recv()
+
     for c in range(chunks):
         for d in ep_order:
-            z_copy[c, d] = send(
+            send(
                 z_out.at[c, rows_of(ep_to(d)), :], z_in.at[c, rows_of(ep), :],
-                s_z_s.at[c, d], s_z_r.at[c, d], {"ep": ep_to(d)})
+                s_z_s.at[c, d], s_z_r.at[c, ep], {"ep": ep_to(d)})
             if c == 0:
-                cnt_copy[d] = send(
+                send(
                     cnt_out.at[ep_to(d)], cnt_in.at[ep],
-                    s_cnt_s.at[d], s_cnt_r.at[d], {"ep": ep_to(d)})
+                    s_cnt_s.at[d], s_cnt_r.at[ep], {"ep": ep_to(d)})
 
     load_aff.wait()
     aff_t = jnp.transpose(aff[...])
@@ -148,7 +159,7 @@
         copy.wait()
 
     for d in ep_order:
-        cnt_copy[d].wait_recv()
+        arrived(cnt_in.at[ep_from(d)], s_cnt_r.at[ep_from(d)])
     lane = lax.broadcasted_iota(jnp.int32, (group, live), 1).astype(F32)
     row = lax.broadcasted_iota(jnp.int32, (group, live), 0).astype(F32)
     start = jnp.zeros((group, live), F32)
@@ -174,7 +185,7 @@
 
     for c in range(chunks):
         for d in ep_order:
-            z_copy[c, d].wait_recv()
+            arrived(z_in.at[c, rows_of(ep_from(d)), :], s_z_r.at[c, ep_from(d)])
         rows[c, tp] = jnp.dot(
             compact[...], z_in[c], preferred_element_type=F32).astype(BF16)
         for o in far:
@@ -182,9 +193,10 @@
                 rows.at[c, tp], rows.at[c, tp],
                 s_x_s.at[c, tp_sem(o)], s_x_r.at[c, tp_sem(o)], {"tp": tp_to(o)})
         take(c, tp)
-        if c > 0:
-            arrivals(c - 1)
-    arrivals(chunks - 1)
+        if c >= LAG:
+            arrivals(c - LAG)
+    for c in range(max(0, chunks - LAG), chunks):
+        arrivals(c)
 
     gate = acc[:, :hidden]
     up = acc[:, hidden:]
@@ -205,7 +217,6 @@
                     part_out.at[c, k], part_in.at[c, tp],
                     s_p_s.at[c, tp_sem(o)], s_p_r.at[c, tp_sem(o)], {"tp": k})
 
-    r_copy = {}
     for c in range(chunks):
         total = part_out[c, tp].astype(F32)
         for o in near:
@@ -214,14 +225,14 @@
         ret_out[c] = jnp.dot(
             expand[...], total.astype(BF16), preferred_element_type=F32).astype(BF16)
         for d in ep_order:
-            r_copy[c, d] = send(
+            send(
                 ret_out.at[c, rows_of(ep_to(d)), :], ret_in.at[c, rows_of(ep), :],
-                s_r_s.at[c, d], s_r_r.at[c, d], {"ep": ep_to(d)})
+                s_r_s.at[c, d], s_r_r.at[c, ep], {"ep": ep_to(d)})
         ret_in[c, rows_of(ep), :] = ret_out[c, rows_of(ep), :]
 
     for c in range(chunks):
         for d in ep_order:
-            r_copy[c, d].wait_recv()
+            arrived(ret_in.at[c, rows_of(ep_from(d)), :], s_r_r.at[c, ep_from(d)])
         back = ret_in[c]
         out_ref[:, c * fc:(c + 1) * fc] = (
             jnp.dot(weight_hi[...], back, preferred_element_type=F32)
@@ -248,7 +259,7 @@
     any_spec = pl.BlockSpec(memory_space=pl.ANY)
     return pl.pallas_call(
         functools.partial(kernel, n_ep, n_tp, chunks),
-        out_shape=jax.ShapeDtypeStruct((n_tok, feats), BF16),
+        out_shape=pltpu.VMEM((n_tok, feats), BF16),
         in_specs=[any_spec] * 6,
         out_specs=pl.BlockSpec(memory_space=pltpu.VMEM),
         scratch_shapes=[

time: 37.2 us -> 33.8 us (0.909)
  Pallas kernels: 35.4 us -> 33 us
  local copies, waits for them, and re-layouts: 1.57 us -> 0.66 us
    pallas_call x1, Pallas kernels: 35.4 us -> 33 us  [per_device(): pl.pallas_call(functools.partial(kernel, n_ep, n_tp, chunks), out_shape=p...]
    unnamed x1, local copies, waits for them, and re-layouts: 1.57 us -> 0.66 us
where the time goes in v2:
time: 33.8 us; the launch traced here: 33.6 us
  Pallas kernels  33 us (98%)
  local copies, waits for them, and re-layouts  0.66 us (2%)
    pallas_call x1, Pallas kernels, per_device(): pl.pallas_call(functools.partial(kernel, n_ep, n_tp, chunks), out_shape=p...  33 us

profile of v2, /device:TPU:0, one launch (start us, length us, event | category | flops | bytes accessed | tf_op | source)
XLA Modules:
  0.0 33.6 jit_solution(3043743095408937198)
XLA Ops:
  0.0 33.0 %shard_map.64 = bf16[128,512]{1,0:T(8,128)(2,1)S(1)} custom-call(bf16[128,2048]{1,0:T(8,128)(2,1)} %tok_hbm.1, s32[8,32]{1,0:T(8,128)} %sel_hbm.1, f32[8,32]{1,0:T(8,128)} %aff_hbm.1, bf16[1,2048,512]{2,1,0:T(8,128)(2,1)} %wg_hbm.1, bf16[1,2048,512]{2,1,0:T(8,128)(2,1)} %wu_hbm.1, bf16[1,512,2048]{2,1,0:T(8,128)(2,1)} %wd_hbm.1), custom_call_target="tpu_custom_call" | custom-call | tf_op jit(solution)/shard_map/pallas_call | solution.py:260
  33.0 0.7 %copy.8 = bf16[128,512]{1,0:T(8,128)(2,1)} copy(bf16[128,512]{1,0:T(8,128)(2,1)S(1)} %shard_map.64) | data formatting | bytes 262144

commit v3 on v2

--- a/solution.py
+++ b/solution.py
@@ -27,7 +27,7 @@
     tok_hbm, sel_hbm, aff_hbm, wg_hbm, wu_hbm, wd_hbm, out_ref,
     tok, sel, aff, wgu, wd, onehot, weight_hi, weight_lo, expand, compact,
     cnt_out, cnt_in, z_out, z_in, rows, acc, hid, part_out, part_in, ret_out, ret_in,
-    s_in, s_wg, s_wu, s_wd, s_cnt_s, s_cnt_r, s_z_s, s_z_r, s_x_s, s_x_r,
+    s_in, s_w, s_cnt_s, s_cnt_r, s_z_s, s_z_r, s_x_s, s_x_r,
     s_p_s, s_p_r, s_r_s, s_r_r,
 ):
     ep = lax.axis_index("ep")
@@ -63,11 +63,11 @@
         up = i + jnp.where(i >= ep, 1, 0)
         return jnp.where(high_half > 0, up, down)
 
-    def ep_from(i):
-        return lax.rem(ep + 1 + i, n_ep)
-
     def rows_of(i):
         return pl.ds(pl.multiple_of(i * group, group), group)
+
+    def cols(k, c):
+        return pl.ds(pl.multiple_of(k * feats + c * fc, 128), fc)
 
     load_sel = pltpu.make_async_copy(sel_hbm, sel, s_in.at[0])
     load_tok = pltpu.make_async_copy(
@@ -84,27 +84,12 @@
         pl.semaphore_signal(barrier, inc=1, device_id={"tp": tp_to(o)}, device_id_type=MESH)
 
     load_aff.start()
-    load_w = []
-    for k in range(n_tp):
-        for c in range(chunks):
-            at = pl.ds(k * feats + c * fc, fc)
-            load_w.append(pltpu.make_async_copy(
-                wg_hbm.at[0, at, :], wgu.at[k, c, :, pl.ds(0, hidden)], s_wg.at[k, c]))
-            load_w.append(pltpu.make_async_copy(
-                wu_hbm.at[0, at, :], wgu.at[k, c, :, pl.ds(hidden, hidden)], s_wu.at[k, c]))
-    load_d = [
-        pltpu.make_async_copy(
-            wd_hbm.at[0, :, pl.ds(k * feats, feats)], wd.at[k], s_wd.at[k])
-        for k in range(n_tp)
-    ]
-    for copy in load_w + load_d:
-        copy.start()
 
     load_sel.wait()
     picked = sel[...].astype(F32)
     count = jnp.sum(jnp.where(picked >= 0, 1.0, 0.0), axis=1, keepdims=True)
     for e in range(n_exp):
-        cnt_out[e] = jnp.broadcast_to(count[e:e + 1, :], (8, 128))
+        cnt_out[e] = jnp.broadcast_to(count[e:e + 1, :], (1, 128))
     picked_t = jnp.transpose(picked)
     token_lane = lax.broadcasted_iota(jnp.int32, (group, n_tok), 1).astype(F32)
     for e in range(n_exp):
@@ -120,30 +105,44 @@
 
     pl.semaphore_wait(barrier, len(ep_order) + len(far))
 
-    sent = []
 
     def send(src, dst, ss, rs, to):
         copy = pltpu.make_async_remote_copy(
             src_ref=src, dst_ref=dst, send_sem=ss, recv_sem=rs,
             device_id=to, device_id_type=MESH)
         copy.start()
-        sent.append(copy)
         return copy
 
-    def arrived(dst, rs):
-        pltpu.make_async_remote_copy(
-            src_ref=dst, dst_ref=dst, send_sem=s_in.at[0], recv_sem=rs,
-            device_id={"ep": ep_from(0)}, device_id_type=MESH).wait_recv()
+    others = (n_ep - 1) * group
+
+    def whole(ref, ss, rs):
+        return pltpu.make_async_remote_copy(
+            src_ref=ref, dst_ref=ref, send_sem=ss, recv_sem=rs,
+            device_id={"ep": ep_to(0)}, device_id_type=MESH)
+
+    cnt_all = whole(cnt_in.at[pl.ds(0, n_ep - 1)], s_cnt_s.at[0], s_cnt_r.at[0])
+    z_all = [
+        whole(z_in.at[c, pl.ds(0, others), :], s_z_s.at[c], s_z_r.at[c]) for c in range(chunks)]
+    r_all = [
+        whole(ret_in.at[c, pl.ds(0, others), :], s_r_s.at[c], s_r_r.at[c]) for c in range(chunks)]
 
     for c in range(chunks):
         for d in ep_order:
             send(
                 z_out.at[c, rows_of(ep_to(d)), :], z_in.at[c, rows_of(ep), :],
-                s_z_s.at[c, d], s_z_r.at[c, ep], {"ep": ep_to(d)})
+                s_z_s.at[c], s_z_r.at[c], {"ep": ep_to(d)})
             if c == 0:
                 send(
                     cnt_out.at[ep_to(d)], cnt_in.at[ep],
-                    s_cnt_s.at[d], s_cnt_r.at[ep], {"ep": ep_to(d)})
+                    s_cnt_s.at[0], s_cnt_r.at[0], {"ep": ep_to(d)})
+
+    load_w = [
+        pltpu.make_async_copy(wg_hbm.at[0], wgu.at[:, pl.ds(0, hidden)], s_w.at[0]),
+        pltpu.make_async_copy(wu_hbm.at[0], wgu.at[:, pl.ds(hidden, hidden)], s_w.at[1]),
+    ]
+    load_d = [pltpu.make_async_copy(wd_hbm.at[0], wd, s_w.at[2])]
+    for copy in load_w + load_d:
+        copy.start()
 
     load_aff.wait()
     aff_t = jnp.transpose(aff[...])
@@ -158,8 +157,7 @@
     for copy in load_w:
         copy.wait()
 
-    for d in ep_order:
-        arrived(cnt_in.at[ep_from(d)], s_cnt_r.at[ep_from(d)])
+    cnt_all.wait_recv()
     lane = lax.broadcasted_iota(jnp.int32, (group, live), 1).astype(F32)
     row = lax.broadcasted_iota(jnp.int32, (group, live), 0).astype(F32)
     start = jnp.zeros((group, live), F32)
@@ -176,7 +174,7 @@
     x_copy = {}
 
     def take(c, k):
-        acc[...] += jnp.dot(rows[c, k], wgu[k, c], preferred_element_type=F32)
+        acc[...] += jnp.dot(rows[c, k], wgu[cols(k, c), :], preferred_element_type=F32)
 
     def arrivals(c):
         for o in near:
@@ -184,8 +182,7 @@
             take(c, tp_from(o))
 
     for c in range(chunks):
-        for d in ep_order:
-            arrived(z_in.at[c, rows_of(ep_from(d)), :], s_z_r.at[c, ep_from(d)])
+        z_all[c].wait_recv()
         rows[c, tp] = jnp.dot(
             compact[...], z_in[c], preferred_element_type=F32).astype(BF16)
         for o in far:
@@ -210,7 +207,7 @@
         for o in far + [(0, 0)]:
             k = tp_to(o)
             part_out[c, k] = jnp.dot(
-                hid[...], wd[k, :, c * fc:(c + 1) * fc], preferred_element_type=F32
+                hid[...], wd[:, cols(k, c)], preferred_element_type=F32
             ).astype(BF16)
             if o != (0, 0):
                 p_copy[c, o] = send(
@@ -227,19 +224,21 @@
         for d in ep_order:
             send(
                 ret_out.at[c, rows_of(ep_to(d)), :], ret_in.at[c, rows_of(ep), :],
-                s_r_s.at[c, d], s_r_r.at[c, ep], {"ep": ep_to(d)})
+                s_r_s.at[c], s_r_r.at[c], {"ep": ep_to(d)})
         ret_in[c, rows_of(ep), :] = ret_out[c, rows_of(ep), :]
 
-    for c in range(chunks):
-        for d in ep_order:
-            arrived(ret_in.at[c, rows_of(ep_from(d)), :], s_r_r.at[c, ep_from(d)])
+    for copy in [cnt_all] + z_all + list(x_copy.values()) + list(p_copy.values()):
+        copy.wait_send()
+
+    for c in range(chunks):
+        r_all[c].wait_recv()
         back = ret_in[c]
         out_ref[:, c * fc:(c + 1) * fc] = (
             jnp.dot(weight_hi[...], back, preferred_element_type=F32)
             + jnp.dot(weight_lo[...], back, preferred_element_type=F32)
         ).astype(BF16)
 
-    for copy in sent:
+    for copy in r_all:
         copy.wait_send()
 
 
@@ -266,15 +265,15 @@
             pltpu.VMEM((n_tok, feats), BF16),
             pltpu.VMEM((n_exp, group), jnp.int32),
             pltpu.VMEM((n_exp, group), F32),
-            pltpu.VMEM((n_tp, chunks, fc, 2 * hidden), BF16),
-            pltpu.VMEM((n_tp, hidden, feats), BF16),
+            pltpu.VMEM((width, 2 * hidden), BF16),
+            pltpu.VMEM((hidden, width), BF16),
             pltpu.VMEM((slots, n_tok), F32),
             pltpu.VMEM((n_tok, slots), BF16),
             pltpu.VMEM((n_tok, slots), BF16),
             pltpu.VMEM((slots, live), BF16),
             pltpu.VMEM((live, slots), BF16),
-            pltpu.VMEM((n_exp, 8, 128), F32),
-            pltpu.VMEM((n_ep, 8, 128), F32),
+            pltpu.VMEM((n_exp, 1, 128), F32),
+            pltpu.VMEM((n_ep, 1, 128), F32),
             pltpu.VMEM((chunks, slots, fc), BF16),
             pltpu.VMEM((chunks, slots, fc), BF16),
             pltpu.VMEM((chunks, n_tp, live, fc), BF16),
@@ -285,19 +284,17 @@
             pltpu.VMEM((chunks, slots, fc), BF16),
             pltpu.VMEM((chunks, slots, fc), BF16),
             dma((3,)),
-            dma((n_tp, chunks)),
-            dma((n_tp, chunks)),
-            dma((n_tp,)),
-            dma((n_ep,)),
-            dma((n_ep,)),
-            dma((chunks, n_ep)),
-            dma((chunks, n_ep)),
+            dma((3,)),
+            dma((1,)),
+            dma((1,)),
+            dma((chunks,)),
+            dma((chunks,)),
             dma((chunks, n_tp)),
             dma((chunks, n_tp)),
             dma((chunks, n_tp)),
             dma((chunks, n_tp)),
-            dma((chunks, n_ep)),
-            dma((chunks, n_ep)),
+            dma((chunks,)),
+            dma((chunks,)),
         ],
         compiler_params=pltpu.CompilerParams(collective_id=0, has_side_effects=True),
     )(tokens, selected, affinity, w_gate, w_up, w_down)

time: 33.8 us -> 31.7 us (0.938)
  Pallas kernels: 33 us -> 30.8 us
    pallas_call x1, Pallas kernels: 33 us -> 30.8 us  [per_device(): pl.pallas_call(functools.partial(kernel, n_ep, n_tp, chunks), out_shape=p...]
where the time goes in v3:
time: 31.7 us; the launch traced here: 31.5 us
  Pallas kernels  30.8 us (97%)
  local copies, waits for them, and re-layouts  0.66 us (2%)
    pallas_call x1, Pallas kernels, per_device(): pl.pallas_call(functools.partial(kernel, n_ep, n_tp, chunks), out_shape=p...  30.8 us
    unnamed x1, local copies, waits for them, and re-layouts  0.66 us

profile of v3, /device:TPU:0, one launch (start us, length us, event | category | flops | bytes accessed | tf_op | source)
XLA Modules:
  0.0 31.5 jit_solution(783534965677840479)
XLA Ops:
  0.0 30.8 %shard_map.64 = bf16[128,512]{1,0:T(8,128)(2,1)S(1)} custom-call(bf16[128,2048]{1,0:T(8,128)(2,1)} %tok_hbm.1, s32[8,32]{1,0:T(8,128)} %sel_hbm.1, f32[8,32]{1,0:T(8,128)} %aff_hbm.1, bf16[1,2048,512]{2,1,0:T(8,128)(2,1)} %wg_hbm.1, bf16[1,2048,512]{2,1,0:T(8,128)(2,1)} %wu_hbm.1, bf16[1,512,2048]{2,1,0:T(8,128)(2,1)} %wd_hbm.1), custom_call_target="tpu_custom_call" | custom-call | tf_op jit(solution)/shard_map/pallas_call | solution.py:259
  30.9 0.7 %copy.8 = bf16[128,512]{1,0:T(8,128)(2,1)} copy(bf16[128,512]{1,0:T(8,128)(2,1)S(1)} %shard_map.64) | data formatting | bytes 262144

commit v4 on v3

--- a/solution.py
+++ b/solution.py
@@ -185,7 +185,7 @@
         z_all[c].wait_recv()
         rows[c, tp] = jnp.dot(
             compact[...], z_in[c], preferred_element_type=F32).astype(BF16)
-        for o in far:
+        for o in near:
             x_copy[c, o] = send(
                 rows.at[c, tp], rows.at[c, tp],
                 s_x_s.at[c, tp_sem(o)], s_x_r.at[c, tp_sem(o)], {"tp": tp_to(o)})
@@ -204,7 +204,7 @@
 
     p_copy = {}
     for c in range(chunks):
-        for o in far + [(0, 0)]:
+        for o in near + [(0, 0)]:
             k = tp_to(o)
             part_out[c, k] = jnp.dot(
                 hid[...], wd[:, cols(k, c)], preferred_element_type=F32

time: 31.7 us -> 31.3 us (0.987)
  Pallas kernels: 30.8 us -> 30.4 us
    pallas_call x1, Pallas kernels: 30.8 us -> 30.4 us  [per_device(): pl.pallas_call(functools.partial(kernel, n_ep, n_tp, chunks), out_shape=p...]
where the time goes in v4:
time: 31.3 us; the launch traced here: 31.1 us
  Pallas kernels  30.4 us (97%)
  local copies, waits for them, and re-layouts  0.66 us (2%)
    pallas_call x1, Pallas kernels, per_device(): pl.pallas_call(functools.partial(kernel, n_ep, n_tp, chunks), out_shape=p...  30.4 us
    unnamed x1, local copies, waits for them, and re-layouts  0.66 us

profile of v4, /device:TPU:0, one launch (start us, length us, event | category | flops | bytes accessed | tf_op | source)
XLA Modules:
  0.0 31.1 jit_solution(14840333539742878817)
XLA Ops:
  0.0 30.4 %shard_map.64 = bf16[128,512]{1,0:T(8,128)(2,1)S(1)} custom-call(bf16[128,2048]{1,0:T(8,128)(2,1)} %tok_hbm.1, s32[8,32]{1,0:T(8,128)} %sel_hbm.1, f32[8,32]{1,0:T(8,128)} %aff_hbm.1, bf16[1,2048,512]{2,1,0:T(8,128)(2,1)} %wg_hbm.1, bf16[1,2048,512]{2,1,0:T(8,128)(2,1)} %wu_hbm.1, bf16[1,512,2048]{2,1,0:T(8,128)(2,1)} %wd_hbm.1), custom_call_target="tpu_custom_call" | custom-call | tf_op jit(solution)/shard_map/pallas_call | solution.py:259
  30.4 0.7 %copy.8 = bf16[128,512]{1,0:T(8,128)(2,1)} copy(bf16[128,512]{1,0:T(8,128)(2,1)S(1)} %shard_map.64) | data formatting | bytes 262144
